TPU v7x, 32 devices: a whole 2x2x4 slice. The times are simulated.
32 devices in a mesh: sp: 8 (over z, y), dp: 4 (over x, core).
Axes of the slice: x: 2, y: 2, z: 4, core: 2. Of those that a mesh axis runs over, the one named last changes fastest.
Arguments:
- out_cotangent: bfloat16 [4, 2048, 2048], P('dp', 'sp'), may hold values from -6 to 6
- value_pre: bfloat16 [4, 2048, 2048], P('dp', 'sp'), may hold values from -8 to 8
- gate_pre: bfloat16 [4, 2048, 2048], P('dp', 'sp'), may hold values from -8 to 8
- out_weight: bfloat16 [2048, 2048], P('dp'), may hold values from -0.125 to 0.125
- conv_kernel: bfloat16 [31, 2048], P(None, 'sp'), may hold values from -6 to 6
- norm_gain: bfloat16 [2048], P('sp'), may hold values from 0.099609375 to 1.8984375
Outputs:
- grad_value: bfloat16 [4, 2048, 2048], P('dp', 'sp')
- grad_gate: bfloat16 [4, 2048, 2048], P('dp', 'sp')
- grad_out_weight: float32 [2048, 2048], P(('sp', 'dp'))
- grad_kernel: float32 [31, 2048], P(None, 'sp')
- grad_gain: float32 [2048], P('sp')
All inputs are finite; a program needn't handle non-finite values.
Results may differ from a plain program's by a relative error of at most 0.011.
Values may be sent and summed in bfloat16 or wider, within the bound.
A program may use at most 128 MiB of HBM per device.

v0:
```python
import jax
import jax.numpy as jnp
from jax import lax
from jax.sharding import PartitionSpec as P

epsilon = 1e-05


def passed_along(value, axis, steps):
    count = lax.axis_size(axis)
    initial, last = (max(0, -steps), min(count, count - steps))
    return lax.ppermute(value, axis, [(source, source + steps) for source in range(initial, last)])


def gated_forward(values_in, gates_in):
    return (values_in.astype(jnp.float32) * jax.nn.sigmoid(gates_in.astype(jnp.float32))).astype(
        jnp.bfloat16
    )


def gated_backward(grad_gated, values_in, gates_in):
    sigmoid_gate = jax.nn.sigmoid(gates_in.astype(jnp.float32))
    grad_float = grad_gated.astype(jnp.float32)
    grad_values = (grad_float * sigmoid_gate).astype(jnp.bfloat16)
    grad_gates = (
        grad_float * values_in.astype(jnp.float32) * sigmoid_gate * (1.0 - sigmoid_gate)
    ).astype(jnp.bfloat16)
    return (grad_values, grad_gates)


def local_sums(first, second):
    return (first, second)


def mechanism(
    gated, front_rows, grad_act, kernel, gain, channel_count, moments_fn, grad_moments_fn, after_fn
):
    taps_count = kernel.shape[0]
    row_count = gated.shape[0]
    taps_float = kernel.astype(jnp.float32)
    gain_float = gain.astype(jnp.float32)
    extended = jnp.concatenate([front_rows, gated], axis=0).astype(jnp.float32)
    conv = jnp.zeros((row_count, gated.shape[1]), jnp.float32)
    for offset in range(taps_count):
        begin = taps_count - 1 - offset
        conv = conv + taps_float[offset] * extended[begin : begin + row_count]
    total, squares = moments_fn(jnp.sum(conv, axis=1), jnp.sum(conv * conv, axis=1))
    centre = (total / channel_count)[:, None]
    variance = (squares / channel_count)[:, None] - centre * centre
    inv_scale = lax.rsqrt(variance + epsilon)
    centred = (conv - centre) * inv_scale
    normed = centred * gain_float
    sig_norm = jax.nn.sigmoid(normed)
    activation = (normed * sig_norm).astype(jnp.bfloat16)
    grad_normed = grad_act.astype(jnp.float32) * sig_norm * (1.0 + normed * (1.0 - sig_norm))
    gain_part = jnp.sum(grad_normed * centred, axis=0)
    grad_centred = grad_normed * gain_float
    first, second = grad_moments_fn(
        jnp.sum(grad_centred, axis=1), jnp.sum(grad_centred * centred, axis=1)
    )
    grad_conv = (
        grad_centred
        - (first / channel_count)[:, None]
        - centred * (second / channel_count)[:, None]
    ) * inv_scale
    grad_extended = jnp.concatenate([grad_conv, after_fn(grad_conv, taps_count)], axis=0)
    grad_gated = jnp.zeros(grad_conv.shape, jnp.float32)
    kernel_rows = []
    for offset in range(taps_count):
        grad_gated = grad_gated + taps_float[offset] * grad_extended[offset : offset + row_count]
        begin = taps_count - 1 - offset
        kernel_rows.append(jnp.sum(grad_conv * extended[begin : begin + row_count], axis=0))
    return (activation, grad_gated.astype(jnp.bfloat16), jnp.stack(kernel_rows, axis=0), gain_part)


def shards(out_cotangent, value_pre, gate_pre, out_weight, conv_kernel, norm_gain):
    cotangent = out_cotangent[0]
    values_in = value_pre[0]
    gates_in = gate_pre[0]
    row_count = cotangent.shape[0]
    taps_count = conv_kernel.shape[0]
    width_all = cotangent.shape[1]
    grad_act = lax.dot_general(
        cotangent,
        lax.all_gather(out_weight, "dp", axis=0, tiled=True),
        (((1,), (1,)), ((), ())),
        preferred_element_type=jnp.float32,
    ).astype(jnp.bfloat16)
    kernel_all, gain_all = (
        lax.all_gather(conv_kernel, "sp", axis=1, tiled=True),
        lax.all_gather(norm_gain, "sp", axis=0, tiled=True),
    )
    gated = gated_forward(values_in, gates_in)
    front_rows = passed_along(gated[row_count - taps_count + 1 :], "sp", 1)

    def later_margin(grad_conv, count_taps):
        return passed_along(grad_conv[: count_taps - 1], "sp", -1)

    activation, grad_gated, kernel_full, gain_full = mechanism(
        gated,
        front_rows,
        grad_act,
        kernel_all,
        gain_all,
        float(width_all),
        local_sums,
        local_sums,
        later_margin,
    )
    kernel_part, gain_part = (
        lax.psum_scatter(kernel_full, "sp", scatter_dimension=1, tiled=True),
        lax.psum_scatter(gain_full, "sp", scatter_dimension=0, tiled=True),
    )
    grad_values, grad_gates = gated_backward(grad_gated, values_in, gates_in)
    token_total = lax.axis_size("sp") * lax.axis_size("dp") * row_count
    factor = float(token_total) ** (-0.5)
    kernel_sum, gain_sum = lax.psum((kernel_part, gain_part), "dp")
    weight_sum = lax.psum_scatter(
        lax.dot_general(
            activation, cotangent, (((0,), (0,)), ((), ())), preferred_element_type=jnp.float32
        ),
        ("sp", "dp"),
        scatter_dimension=0,
        tiled=True,
    )
    return (
        grad_values[None],
        grad_gates[None],
        weight_sum * factor,
        kernel_sum * factor,
        gain_sum * factor,
    )


def solution(mesh):
    placed = (
        P("dp", "sp", None),
        P("dp", "sp", None),
        P("dp", "sp", None),
        P("dp", None),
        P(None, "sp"),
        P("sp"),
    )
    return jax.shard_map(
        shards,
        mesh=mesh,
        in_specs=placed,
        out_specs=(
            P("dp", "sp", None),
            P("dp", "sp", None),
            P(("sp", "dp"), None),
            P(None, "sp"),
            P("sp"),
        ),
        check_vma=False,
    )
```

profile of v0, /device:TPU:14, one launch (start us, length us, event | category | flops | bytes accessed | tf_op | source)
XLA Modules:
  0.0 356.1 jit_solution(7777059635659343137)
XLA Ops:
  7.3 0.7 all-gather.3.cloned.1.call-update
  9.4 3.4 collective-permute-start
  12.9 25.9 %all_gather.9 = bf16[31,2048]{1,0:T(8,128)(2,1)S(1)} all-gather(bf16[31,256]{1,0:T(8,128)(2,1)S(1)} %copy-done.24), channel_id=1, replica_groups=mesh['sp'=8,'dp'=4] {'sp'}, dimensions={1}, use_global_device_ids=true | all-gather | bytes 142848 | tf_op jit(solution)/shard_map/all_gather | solution.py:90
  39.1 19.0 %all-gather = bf16[8,1,256]{2,1,0:T(2,128)(2,1)S(1)} all-gather(bf16[1,1,256]{2,1,0:T(2,128)(2,1)S(1)} %reshape.43), channel_id=1, replica_groups=mesh['sp'=8,'dp'=4] {'sp'}, dimensions={0}, use_global_device_ids=true | all-gather | bytes 4608 | tf_op jit(solution)/shard_map/all_gather | solution.py:91
  58.5 11.8 %fusion.108 = (f32[256]{0:T(256)S(1)}, f32[256]{0:T(256)S(1)}, f32[256,2048]{1,0:T(8,128)}) fusion(f32[286,2048]{1,0:T(8,128)S(1)} %maximum_convert_fusion, f32[2048]{0:T(1024)S(1)} %bitcast.154, f32[2048]{0:T(1024)S(1)} %bitcast.152, f32[2048]{0:T(1024)S(1)} %bitcast.150, f32[2048]{0:T(1024)S(1)} %bitcast.148, f32[2048]{0:T(1024)S(1)} %bitcast.146, ...), kind=kLoop, calls=%fused_computation.221 | loop fusion | flops 33553920 | bytes 67364864 | tf_op jit(solution)/shard_map/reduce_sum | solution.py:47
  70.4 0.6 broadcast_multiply_fusion.5
  71.0 8.1 %multiply_reduce_fusion = (f32[2048]{0:T(1024)}, f32[256]{0:T(256)S(1)}, f32[256]{0:T(256)S(1)}, f32[256,2048]{1,0:T(8,128)S(1)}) fusion(f32[256,2048]{1,0:T(8,128)} %get-tuple-element.46, f32[256]{0:T(256)} %get-tuple-element.79, f32[256]{0:T(256)} %get-tuple-element.78, f32[2048]{0:T(1024)S(1)} %bitcast.91, ...), kind=kOutput, calls=%fused_computation.162 | convolution fusion | flops 2157442560 | bytes 13651968 | tf_op jit(solution)/shard_map/dot_general | solution.py:83
  79.1 6.8 %multiply_reduce_fusion.1 = (f32[2048]{0:T(1024)}, f32[2048]{0:T(1024)}, f32[2048]{0:T(1024)}, f32[2048]{0:T(1024)}, f32[2048]{0:T(1024)}, /*index=5*/f32[2048]{...) fusion(f32[286,2048]{1,0:T(8,128)S(1)} %maximum_convert_fusion,, ...), kind=kLoop, calls=%fused_computation.163 | loop fusion | flops 22507520 | bytes 44199936 | tf_op jit(solution)/shard_map/reduce_sum | solution.py:72
  85.9 4.8 %multiply_reduce_fusion.19 = (f32[2048]{0:T(1024)}, f32[2048]{0:T(1024)}, f32[2048]{0:T(1024)}, f32[2048]{0:T(1024)}, f32[2048]{0:T(1024)}, /*index=5*/f32[2048]...) fusion(f32[256,2048]{1,0:T(8,128)S(1)} %get-tuple-element.43, ...), kind=kLoop, calls=%fused_computation.181 | loop fusion | flops 13604864 | bytes 29466624 | tf_op jit(solution)/shard_map/reduce_sum | solution.py:72
  90.7 6.1 %stack.127 = f32[31,2048]{1,0:T(8,128)} concatenate(f32[1,2048]{1,0:T(1,128)} %bitcast.186, f32[1,2048]{1,0:T(1,128)} %bitcast.185, f32[1,2048]{1,0:T(1,128)} %bitcast.184, f32[1,2048]{1,0:T(1,128)} %bitcast.183, f32[1,2048]{1,0:T(1,128)} %bitcast.182, f32[1,2048]{1,0:T(1,128)} %bitcast.181, f32[1,2048]{1,0:T(1,128)} %bitcast.180, f32[1,2048]{1,0:T(1,128)} %bitcast.179, ...), dimensions={0} | concatenate | bytes 507904 | tf_op jit(solution)/shard_map/stack | solution.py:73
  97.1 10.0 %fusion.98 = f32[2048,2048]{1,0:T(8,128)} fusion(f32[256,2048]{1,0:T(8,128)} %get-tuple-element.46, bf16[1,256,2048]{2,1,0:T(8,128)(2,1)S(1)} %copy-done, f32[2048]{0:T(1024)S(1)} %bitcast.93, f32[256]{0:T(256)} %get-tuple-element.79, f32[256]{0:T(256)} %get-tuple-element.78), kind=kOutput, calls=%fused_computation.204 | convolution fusion | flops 2151677952 | bytes 19933184 | tf_op jit(solution)/shard_map/dot_general | solution.py:119
  107.1 1.6 copy-done.2
  108.7 3.9 %collective-permute-start.1 = (f32[30,2048]{1,0:T(8,128)S(1)}, f32[30,2048]{1,0:T(8,128)}, u32[]{:S(2)}, u32[]{:S(2)}) collective-permute-start(f32[30,2048]{1,0:T(8,128)S(1)} %slice.501), channel_id=1, source_target_pairs={{4,0},{8,4},{12,8},{16,12},{20,16},{24,20},{28,24},{5,1},{9,5},{13... | collective-permute-start | bytes 737288 | tf_op jit(solution)/shard_map/ppermute | solution.py:12
  112.6 1.2 dynamic-slice
  114.5 17.5 %all-reduce = f32[2048]{0:T(1024)} all-reduce(f32[2048]{0:T(1024)} %get-tuple-element.36), channel_id=4, replica_groups=mesh['sp'=8,'dp'=4] {'sp'}, use_global_device_ids=true, to_apply=%region_39.0.clone | all-reduce | flops 2048 | bytes 16384
  132.0 1.3 dynamic-slice.1
  133.3 18.0 %fusion.99 = (bf16[1,256,2048]{2,1,0:T(8,128)(2,1)}, bf16[256,2048]{1,0:T(8,128)(2,1)S(1)}) fusion(bf16[1,256,2048]{2,1,0:T(8,128)(2,1)} %param.7, bf16[1,256,2048]{2,1,0:T(8,128)(2,1)} %param.8, f32[30,2048]{1,0:T(8,128)} %collective-permute-done.1, f32[256,2048]{1,0:T(8,128)S(1)} %copy-done.2, f32[2048]{0:T(1024)} %bitcast.155, f32[2048]{0:T(1024)} %bitcast.153, ...), kind=kLoop, calls=%fused_computation.205 | loop fusion | flops 54001664 | bytes 6791168 | tf_op jit(solution)/shard_map/broadcast_in_dim | solution.py:128
  151.4 1.6 fusion.100
  153.0 8.0 %reduce-scatter.5.cloned.1.call-done = f32[31,256]{1,0:T(8,128)} async-done(((f32[31,2048]{1,0:T(8,128)}), f32[31,256]{1,0:T(8,128)}) %reduce-scatter.5.cloned.1.call-update) | async-done | bytes 31760 | tf_op jit(solution)/shard_map/reduce_scatter | solution.py:111
  160.9 14.4 %all-reduce.1 = (f32[31,256]{1,0:T(8,128)S(1)}, f32[256]{0:T(256)S(1)}) all-reduce(f32[31,256]{1,0:T(8,128)} %reduce-scatter.5.cloned.1.call-done, f32[256]{0:T(256)S(1)} %copy-done.25), channel_id=1, replica_groups=mesh['sp'=8,'dp'=4] {'dp'}, use_global_device_ids=true, to_apply=%region_37.0 | all-reduce | flops 8192 | bytes 65536 | tf_op jit(solution)/shard_map/psum | solution.py:117
  175.3 0.6 broadcast_multiply_fusion.2
  175.9 0.6 broadcast_multiply_fusion.1
  176.5 171.1 %reduce-scatter.3.cloned.1.call-done = f32[64,2048]{1,0:T(8,128)} async-done(((f32[2048,2048]{1,0:T(8,128)}), f32[64,2048]{1,0:T(8,128)}) %reduce-scatter.3.cloned.1.call-update) | async-done | bytes 524304 | tf_op jit(solution)/shard_map/reduce_scatter | solution.py:118
  347.6 1.9 broadcast_multiply_fusion
  (70 shorter events, 2.4 us)
Async XLA Ops:
  7.2 63.8 %copy-start = (bf16[1,256,2048]{2,1,0:T(8,128)(2,1)S(1)}, bf16[1,256,2048]{2,1,0:T(8,128)(2,1)}, u32[]{:S(2)}) copy-start(bf16[1,256,2048]{2,1,0:T(8,128)(2,1)} %param.6) | copy-start | bytes 3145732
  7.2 63.8 %all-gather.3.cloned.1.call-start = ((), (), s32[]{:S(2)}) async-start(), calls=%async_computation.2 | async-start | bytes 10485760 | tf_op jit(solution)/shard_map/all_gather | solution.py:85
  8.0 31.0 %copy-start.26 = (bf16[256]{0:T(256)(128)(2,1)S(1)}, bf16[256]{0:T(256)(128)(2,1)}, u32[]{:S(2)}) copy-start(bf16[256]{0:T(256)(128)(2,1)} %param.11) | copy-start | bytes 1540
  8.0 153.0 %reduce-scatter.5.cloned.1.call-start = ((), (), s32[]{:S(2)}) async-start(), calls=%async_computation.4 | async-start | bytes 294912 | tf_op jit(solution)/shard_map/reduce_scatter | solution.py:111
  9.4 48.7 %collective-permute-start = (bf16[30,2048]{1,0:T(8,128)(2,1)S(1)}, bf16[30,2048]{1,0:T(8,128)(2,1)S(1)}, u32[]{:S(2)}, u32[]{:S(2)}) collective-permute-start(bf16[30,2048]{1,0:T(8,128)(2,1)S(1)} %slice.439), channel_id=1, source_target_pairs={{0,4},{4,8},{8,12},{12,16},{16,20},{20,24},{24,28},{1,5},{5,9},{9,... | collective-permute-start | bytes 368648 | tf_op jit(solution)/shard_map/ppermute | solution.py:12
  38.9 31.4 %copy-start.7 = (f32[1,2048]{1,0:T(1,128)}, f32[1,2048]{1,0:T(1,128)S(1)}, u32[]{:S(2)}) copy-start(f32[1,2048]{1,0:T(1,128)S(1)} %get-tuple-element.64) | copy-start | bytes 24580
  38.9 31.4 %copy-start.9 = (f32[1,2048]{1,0:T(1,128)}, f32[1,2048]{1,0:T(1,128)S(1)}, u32[]{:S(2)}) copy-start(f32[1,2048]{1,0:T(1,128)S(1)} %get-tuple-element.65) | copy-start | bytes 24580
  39.0 31.3 %copy-start.10 = (f32[1,2048]{1,0:T(1,128)}, f32[1,2048]{1,0:T(1,128)S(1)}, u32[]{:S(2)}) copy-start(f32[1,2048]{1,0:T(1,128)S(1)} %get-tuple-element.66) | copy-start | bytes 24580
  39.0 31.3 %copy-start.11 = (f32[1,2048]{1,0:T(1,128)}, f32[1,2048]{1,0:T(1,128)S(1)}, u32[]{:S(2)}) copy-start(f32[1,2048]{1,0:T(1,128)S(1)} %get-tuple-element.67) | copy-start | bytes 24580
  39.0 31.3 %copy-start.12 = (f32[1,2048]{1,0:T(1,128)}, f32[1,2048]{1,0:T(1,128)S(1)}, u32[]{:S(2)}) copy-start(f32[1,2048]{1,0:T(1,128)S(1)} %get-tuple-element.68) | copy-start | bytes 24580
  39.0 31.3 %copy-start.13 = (f32[1,2048]{1,0:T(1,128)}, f32[1,2048]{1,0:T(1,128)S(1)}, u32[]{:S(2)}) copy-start(f32[1,2048]{1,0:T(1,128)S(1)} %get-tuple-element.69) | copy-start | bytes 24580
  39.0 31.3 %copy-start.14 = (f32[1,2048]{1,0:T(1,128)}, f32[1,2048]{1,0:T(1,128)S(1)}, u32[]{:S(2)}) copy-start(f32[1,2048]{1,0:T(1,128)S(1)} %get-tuple-element.70) | copy-start | bytes 24580
  39.0 31.3 %copy-start.15 = (f32[1,2048]{1,0:T(1,128)}, f32[1,2048]{1,0:T(1,128)S(1)}, u32[]{:S(2)}) copy-start(f32[1,2048]{1,0:T(1,128)S(1)} %get-tuple-element.71) | copy-start | bytes 24580
  39.1 31.3 %copy-start.16 = (f32[1,2048]{1,0:T(1,128)}, f32[1,2048]{1,0:T(1,128)S(1)}, u32[]{:S(2)}) copy-start(f32[1,2048]{1,0:T(1,128)S(1)} %get-tuple-element.72) | copy-start | bytes 24580
  39.1 31.3 %copy-start.17 = (f32[1,2048]{1,0:T(1,128)}, f32[1,2048]{1,0:T(1,128)S(1)}, u32[]{:S(2)}) copy-start(f32[1,2048]{1,0:T(1,128)S(1)} %get-tuple-element.73) | copy-start | bytes 24580
  39.1 31.3 %copy-start.18 = (f32[1,2048]{1,0:T(1,128)}, f32[1,2048]{1,0:T(1,128)S(1)}, u32[]{:S(2)}) copy-start(f32[1,2048]{1,0:T(1,128)S(1)} %get-tuple-element.74) | copy-start | bytes 24580
  39.1 31.3 %copy-start.19 = (f32[1,2048]{1,0:T(1,128)}, f32[1,2048]{1,0:T(1,128)S(1)}, u32[]{:S(2)}) copy-start(f32[1,2048]{1,0:T(1,128)S(1)} %get-tuple-element.75) | copy-start | bytes 24580
  39.1 31.3 %copy-start.20 = (f32[1,2048]{1,0:T(1,128)}, f32[1,2048]{1,0:T(1,128)S(1)}, u32[]{:S(2)}) copy-start(f32[1,2048]{1,0:T(1,128)S(1)} %get-tuple-element.76) | copy-start | bytes 24580
  39.1 31.3 %copy-start.21 = (f32[1,2048]{1,0:T(1,128)}, f32[1,2048]{1,0:T(1,128)S(1)}, u32[]{:S(2)}) copy-start(f32[1,2048]{1,0:T(1,128)S(1)} %get-tuple-element.77) | copy-start | bytes 24580
  96.9 250.8 %reduce-scatter.3.cloned.1.call-start = ((), (), s32[]{:S(2)}) async-start(), calls=%async_computation.3 | async-start | bytes 17301504 | tf_op jit(solution)/shard_map/reduce_scatter | solution.py:118
  107.1 26.2 %copy-start.8 = (f32[1,2048]{1,0:T(1,128)S(1)}, f32[1,2048]{1,0:T(1,128)}, u32[]{:S(2)}) copy-start(f32[1,2048]{1,0:T(1,128)} %copy-done.7) | copy-start | bytes 24580
  108.7 24.6 %collective-permute-start.1 = (f32[30,2048]{1,0:T(8,128)S(1)}, f32[30,2048]{1,0:T(8,128)}, u32[]{:S(2)}, u32[]{:S(2)}) collective-permute-start(f32[30,2048]{1,0:T(8,128)S(1)} %slice.501), channel_id=1, source_target_pairs={{4,0},{8,4},{12,8},{16,12},{20,16},{24,20},{28,24},{5,1},{9,5},{13... | collective-permute-start | bytes 737288 | tf_op jit(solution)/shard_map/ppermute | solution.py:12
  133.3 18.1 %copy-start.5 = (bf16[1,256,2048]{2,1,0:T(8,128)(2,1)S(1)}, bf16[1,256,2048]{2,1,0:T(8,128)(2,1)}, u32[]{:S(2)}) copy-start(bf16[1,256,2048]{2,1,0:T(8,128)(2,1)} %param.8) | copy-start | bytes 3145732
  151.4 9.6 %copy-start.25 = (f32[256]{0:T(256)S(1)}, f32[256]{0:T(256)}, u32[]{:S(2)}) copy-start(f32[256]{0:T(256)} %dynamic-slice.1) | copy-start | bytes 3076
  (8 other events, 38.6 us)
Sparse Core Ops, SparseCore 0:
  9.6 58.4 all-gather.2
  97.0 63.9 reduce-scatter.4
  163.2 184.3 reduce-scatter.2
where the time goes:
time: 357 us; the launch traced here: 356 us
  waiting for transfers between devices  180 us (50%)
  blocking collectives  76.8 us (22%)
  other arithmetic  47.5 us (13%)
  matrix products  18.1 us (5%)
  between operations  14.8 us (4%)
  local copies, waits for them, and re-layouts  11.4 us (3%)
  starting transfers between devices  7.62 us (2%)
    reduce_scatter x1, waiting for transfers between devices, shards(): lax.psum_scatter(lax.dot_general(activation, cotangent, (((0,), (0,)), ((...  171 us
    all_gather x1, blocking collectives, shards(): lax.all_gather(conv_kernel, 'sp', axis=1, tiled=True)  25.9 us
    all_gather x1, blocking collectives, shards(): lax.all_gather(norm_gain, 'sp', axis=0, tiled=True)  19 us
    broadcast_in_dim x1, other arithmetic, shards(): grad_gates[None]  18 us
    unnamed x1, blocking collectives  17.5 us
    psum x1, blocking collectives, shards(): kernel_sum, gain_sum = lax.psum((kernel_part, gain_part), 'dp')  14.4 us
    reduce_sum x1, other arithmetic, mechanism(): jnp.sum(conv, axis=1)  11.8 us
    reduce_sum x2, other arithmetic, mechanism(): jnp.sum(grad_conv * extended[begin:begin + row_count], axis=0)  11.6 us
  transfers between devices with their start and end apart: 5, of which 2 were waited for; matrix products, arithmetic and copies ran while one was open for 13% of the time, Pallas kernels for 0%

commit v1 on v0

v1 whole, which is shorter than its diff:
```python
import functools

import jax
import jax.numpy as jnp
from jax import lax
from jax.experimental import pallas as pl
from jax.experimental.pallas import tpu as pltpu
from jax.sharding import PartitionSpec as P

epsilon = 1e-05
LANES = 128
HALVES = 2
f32 = jnp.float32
bf16 = jnp.bfloat16


def block_kernel(
    S, N, T, C, K, HB, ids,
    cot, val, gate, w, taps,
    gv, gg, gw, kout,
    cot_all, ext, cen, gc, gext, kall, act, act_all, ga_send, ga, wpart, rbuf,
    kg, krecv, ksum, k2recv, send_sem, recv_sem,
):
    s = lax.axis_index("sp")
    d = lax.axis_index("dp")
    chunks = C // LANES
    cps = chunks // S
    cpd = chunks // N
    block = C // (S * N)
    RB = min(T, 128)
    total = S * N
    me = s * N + d
    partner = d + 1 - 2 * lax.rem(d, 2)
    factor = float(S * N * T) ** (-0.5)
    hrows = T // HALVES
    waits = []

    def copy(src, dst, i, to_s, to_d):
        return pltpu.make_async_remote_copy(
            src_ref=src, dst_ref=dst, send_sem=send_sem.at[i], recv_sem=recv_sem.at[i],
            device_id={"sp": to_s, "dp": to_d}, device_id_type=pl.DeviceIdType.MESH,
        )

    def send(src, dst, i, to_s, to_d):
        c = copy(src, dst, i, to_s, to_d)
        c.start()
        waits.append(c)

    def arrived(dst, i):
        copy(dst, dst, i, s, partner).wait_recv()

    barrier = pltpu.get_barrier_semaphore()

    def greet(j, _):
        other = lax.rem(me + j, total)
        pl.semaphore_signal(
            barrier, inc=1, device_id={"sp": other // N, "dp": lax.rem(other, N)},
            device_id_type=pl.DeviceIdType.MESH,
        )
        return _

    lax.fori_loop(1, total, greet, 0)
    def gate_chunk(cb, _):
        cols = pl.ds(pl.multiple_of(cb * LANES, LANES), LANES)
        sig = jax.nn.sigmoid(gate[:, cols].astype(f32))
        ext[cb, pl.ds(HB, T), :] = (val[:, cols].astype(f32) * sig).astype(bf16).astype(f32)
        return _

    lax.fori_loop(0, chunks, gate_chunk, 0)
    pl.semaphore_wait(barrier, total - 1)

    for j in range(1, S):
        send(taps, kall.at[pl.ds(s * cps, cps)], ids["taps"] + j, lax.rem(s + j, S), d)
    following = lax.rem(s + 1, S)
    preceding = lax.rem(s + S - 1, S)
    send(ext.at[:, pl.ds(T, HB), :], ext.at[:, pl.ds(0, HB), :], ids["front"], following, d)
    for j in range(1, N // 2):
        for h in range(HALVES):
            rows = pl.ds(h * hrows, hrows)
            send(cot.at[rows], cot_all.at[d, rows], ids["mirror"] + j * HALVES + h, s, lax.rem(d + 2 * j, N))
    send(cot, cot_all.at[d], ids["partner"], s, partner)
    kall[pl.ds(s * cps, cps)] = taps[...]
    cot_all[d] = cot[...]
    for j in range(1, S):
        arrived(kall.at[pl.ds(lax.rem(s + S - j, S) * cps, cps)], ids["taps"] + j)
    arrived(ext.at[:, pl.ds(0, HB), :], ids["front"])

    @pl.when(s == 0)
    def _():
        ext[:, pl.ds(0, HB), :] = jnp.zeros((chunks, HB, LANES), f32)

    def conv_chunk(cb, sums):
        tf = kall[cb].astype(f32)
        parts = []
        for rb in range(T // RB):
            acc = jnp.zeros((RB, LANES), f32)
            for k in range(K):
                acc = acc + tf[k : k + 1] * ext[cb, pl.ds(HB - k + rb * RB, RB), :]
            cen[cb, pl.ds(rb * RB, RB), :] = acc
            parts.append(jnp.sum(acc, axis=1, keepdims=True))
        return sums + jnp.concatenate(parts, axis=0)

    column = jnp.zeros((T, 1), f32)
    mean = lax.fori_loop(0, chunks, conv_chunk, column) / C

    def square_chunk(cb, sums):
        dev = cen[cb] - mean
        return sums + dev * dev

    squares = lax.fori_loop(0, chunks, square_chunk, jnp.zeros((T, LANES), f32))
    inv = lax.rsqrt(jnp.sum(squares, axis=1, keepdims=True) / C + epsilon)

    def relay():
        for j in range(1, N // 2):
            origin = lax.rem(d + N - 2 * j, N)
            for h in range(HALVES):
                piece = cot_all.at[origin, pl.ds(h * hrows, hrows)]
                arrived(piece, ids["mirror"] + j * HALVES + h)
                send(piece, piece, ids["relay"] + j * HALVES + h, s, partner)

    def act_chunk(cb, _):
        centred = (cen[cb] - mean) * inv
        cen[cb] = centred
        normed = centred * kall[cb].astype(f32)[K : K + 1]
        act[cb] = (normed * jax.nn.sigmoid(normed)).astype(bf16)
        return _

    lax.fori_loop(0, chunks, act_chunk, 0)
    for j in range(1, N):
        to = lax.rem(d + j, N)
        send(act.at[pl.ds(to * cpd, cpd)], act_all.at[d], ids["act"] + j, s, to)
    act_all[d] = act[pl.ds(d * cpd, cpd)]

    def project(source, slot):
        def pair(m, _):
            rows = pl.ds(pl.multiple_of(m * 2 * LANES, 2 * LANES), 2 * LANES)
            out = lax.dot_general(
                cot_all[source], w[rows, :], (((1,), (1,)), ((), ())), preferred_element_type=f32
            ).astype(bf16)
            ga_send[slot, 2 * m] = out[:, :LANES]
            ga_send[slot, 2 * m + 1] = out[:, LANES:]
            return _

        lax.fori_loop(0, cpd // 2, pair, 0)

    mine = pl.ds(d * cpd, cpd)
    project(d, 0)
    ga[mine] = ga_send[0]
    arrived(cot_all.at[partner], ids["partner"])
    project(partner, 1)
    send(ga_send.at[1], ga.at[mine], ids["ga"] + 1, s, partner)
    relay()
    for j in range(1, N // 2):
        origin = lax.rem(d + N - 2 * j, N)
        project(origin, 2 * j)
        send(ga_send.at[2 * j], ga.at[mine], ids["ga"] + 2 * j, s, origin)
    for j in range(1, N // 2):
        origin = lax.rem(partner + N - 2 * j, N)
        for h in range(HALVES):
            arrived(cot_all.at[origin, pl.ds(h * hrows, hrows)], ids["relay"] + j * HALVES + h)
        project(origin, 2 * j + 1)
        send(ga_send.at[2 * j + 1], ga.at[mine], ids["ga"] + 2 * j + 1, s, origin)

    for j in range(1, N):
        arrived(act_all.at[lax.rem(d + N - j, N)], ids["act"] + j)
    NT = min(C, 512)

    def weight_tile(i, _):
        m, n = i // (C // NT), lax.rem(i, C // NT)
        cols = pl.ds(pl.multiple_of(n * NT, NT), NT)
        acc = jnp.zeros((LANES, NT), f32)
        for q in range(N):
            acc = acc + lax.dot_general(
                act_all[q, m], cot_all[q, :, cols], (((0,), (0,)), ((), ())),
                preferred_element_type=f32,
            )
        wpart[pl.ds(pl.multiple_of(m * LANES, LANES), LANES), cols] = acc.astype(bf16)
        return _

    lax.fori_loop(0, cpd * (C // NT), weight_tile, 0)

    def block_of(j):
        i = lax.rem(s + j, S)
        owner = d * S + i
        rows = pl.ds(pl.multiple_of(i * block, block), block)
        return owner, rows, pltpu.make_async_remote_copy(
            src_ref=wpart.at[rows], dst_ref=rbuf.at[s], send_sem=send_sem.at[ids["rs"] + j],
            recv_sem=recv_sem.at[ids["rs"] + s],
            device_id={"sp": owner // N, "dp": lax.rem(owner, N)},
            device_id_type=pl.DeviceIdType.MESH,
        )

    for j in range(S):
        owner, rows, c = block_of(j)

        @pl.when(owner != me)
        def _():
            c.start()

        @pl.when(owner == me)
        def _():
            rbuf[s] = wpart[rows, :]

    for j in range(1, N // 2):
        arrived(ga.at[pl.ds(lax.rem(d + 2 * j, N) * cpd, cpd)], ids["ga"] + 2 * j)
        arrived(ga.at[pl.ds(lax.rem(partner + 2 * j, N) * cpd, cpd)], ids["ga"] + 2 * j + 1)
    arrived(ga.at[pl.ds(partner * cpd, cpd)], ids["ga"] + 1)

    def grad_chunk(cb, sums):
        one, two = sums
        centred = cen[cb]
        gain = kall[cb].astype(f32)[K : K + 1]
        normed = centred * gain
        sg = jax.nn.sigmoid(normed)
        grad = ga[cb].astype(f32) * sg * (1.0 + normed * (1.0 - sg))
        kg[cb, pl.ds(K, 1), :] = jnp.sum(grad * centred, axis=0, keepdims=True)
        grad = grad * gain
        gc[cb] = grad
        return one + grad, two + grad * centred

    zero = jnp.zeros((T, LANES), f32)
    one, two = lax.fori_loop(0, chunks, grad_chunk, (zero, zero))
    first = jnp.sum(one, axis=1, keepdims=True) / C
    second = jnp.sum(two, axis=1, keepdims=True) / C

    def conv_grad(cb, _):
        gext[cb, pl.ds(0, T), :] = (gc[cb] - first - cen[cb] * second) * inv
        return _

    lax.fori_loop(0, chunks, conv_grad, 0)
    send(gext.at[:, pl.ds(0, HB), :], gext.at[:, pl.ds(T, HB), :], ids["back"], preceding, d)

    def taps_chunk(cb, _):
        for k in range(K):
            acc = jnp.zeros((8, LANES), f32)
            for rb in range(T // RB):
                prod = gext[cb, pl.ds(rb * RB, RB), :] * ext[cb, pl.ds(HB - k + rb * RB, RB), :]
                acc = acc + jnp.sum(prod.reshape(RB // 8, 8, LANES), axis=0)
            kg[cb, pl.ds(k, 1), :] = jnp.sum(acc, axis=0, keepdims=True)
        return _

    lax.fori_loop(0, chunks, taps_chunk, 0)
    for j in range(1, S):
        to = lax.rem(s + j, S)
        send(kg.at[pl.ds(to * cps, cps)], krecv.at[j], ids["kg"] + j, to, d)

    arrived(gext.at[:, pl.ds(T, HB), :], ids["back"])

    @pl.when(s == S - 1)
    def _():
        gext[:, pl.ds(T, HB), :] = jnp.zeros((chunks, HB, LANES), f32)

    def gated_chunk(cb, _):
        cols = pl.ds(pl.multiple_of(cb * LANES, LANES), LANES)
        tf = kall[cb].astype(f32)
        for rb in range(T // RB):
            rows = pl.ds(rb * RB, RB)
            acc = jnp.zeros((RB, LANES), f32)
            for k in range(K):
                acc = acc + tf[k : k + 1] * gext[cb, pl.ds(k + rb * RB, RB), :]
            acc = acc.astype(bf16).astype(f32)
            sig = jax.nn.sigmoid(gate[rows, cols].astype(f32))
            gv[rows, cols] = (acc * sig).astype(bf16)
            gg[rows, cols] = (acc * val[rows, cols].astype(f32) * sig * (1.0 - sig)).astype(bf16)
        return _

    lax.fori_loop(0, chunks, gated_chunk, 0)

    acc = kg[pl.ds(s * cps, cps)]
    for j in range(1, S):
        arrived(krecv.at[j], ids["kg"] + j)
        acc = acc + krecv[j]
    ksum[...] = acc
    for j in range(1, N):
        send(ksum, k2recv.at[j], ids["k2"] + j, s, lax.rem(d + j, N))
    for j in range(1, N):
        arrived(k2recv.at[j], ids["k2"] + j)
        acc = acc + k2recv[j]
    kout[...] = acc * factor

    home = me // S
    for q in range(S):
        @pl.when(jnp.logical_or(q != s, home != d))
        def _():
            arrived(rbuf.at[q], ids["rs"] + q)

    def sum_tile(n, _):
        cols = pl.ds(pl.multiple_of(n * LANES, LANES), LANES)
        acc = rbuf[0, :, cols].astype(f32)
        for q in range(1, S):
            acc = acc + rbuf[q, :, cols].astype(f32)
        gw[:, cols] = acc * factor
        return _

    lax.fori_loop(0, chunks, sum_tile, 0)
    for j in range(S):
        owner, rows, c = block_of(j)

        @pl.when(owner != me)
        def _():
            c.wait_send()

    for c in waits:
        c.wait_send()


def shards(out_cotangent, value_pre, gate_pre, out_weight, conv_kernel, norm_gain):
    S, N = lax.axis_size("sp"), lax.axis_size("dp")
    _, T, C = out_cotangent.shape
    K = conv_kernel.shape[0]
    chunks, cps, cpd, block = C // LANES, C // LANES // S, C // LANES // N, C // (S * N)
    HB = -(-(K - 1) // 16) * 16
    KP = -(-(K + 1) // 16) * 16
    packed = jnp.concatenate(
        [conv_kernel, norm_gain[None], jnp.zeros((KP - K - 1, C // S), bf16)], axis=0
    )
    packed = jnp.transpose(packed.reshape(KP, cps, LANES), (1, 0, 2))
    ids, count = {}, 0
    for name, size in (
        ("taps", S), ("front", 1), ("back", 1), ("partner", 1), ("mirror", N // 2 * HALVES),
        ("relay", N // 2 * HALVES), ("act", N), ("ga", N), ("rs", S), ("kg", S), ("k2", N),
    ):
        ids[name] = count
        count += size
    vm = pl.BlockSpec(memory_space=pltpu.VMEM)
    grad_value, grad_gate, grad_weight, small = pl.pallas_call(
        functools.partial(block_kernel, S, N, T, C, K, HB, ids),
        out_shape=(
            jax.ShapeDtypeStruct((T, C), bf16),
            jax.ShapeDtypeStruct((T, C), bf16),
            jax.ShapeDtypeStruct((block, C), f32),
            jax.ShapeDtypeStruct((cps, KP, LANES), f32),
        ),
        in_specs=[vm] * 5,
        out_specs=(vm,) * 4,
        scratch_shapes=[
            pltpu.VMEM((N, T, C), bf16),
            pltpu.VMEM((chunks, T + HB, LANES), f32),
            pltpu.VMEM((chunks, T, LANES), f32),
            pltpu.VMEM((chunks, T, LANES), f32),
            pltpu.VMEM((chunks, T + HB, LANES), f32),
            pltpu.VMEM((chunks, KP, LANES), bf16),
            pltpu.VMEM((chunks, T, LANES), bf16),
            pltpu.VMEM((N, cpd, T, LANES), bf16),
            pltpu.VMEM((N, cpd, T, LANES), bf16),
            pltpu.VMEM((chunks, T, LANES), bf16),
            pltpu.VMEM((cpd * LANES, C), bf16),
            pltpu.VMEM((S, block, C), bf16),
            pltpu.VMEM((chunks, KP, LANES), f32),
            pltpu.VMEM((S, cps, KP, LANES), f32),
            pltpu.VMEM((cps, KP, LANES), f32),
            pltpu.VMEM((N, cps, KP, LANES), f32),
            pltpu.SemaphoreType.DMA((count,)),
            pltpu.SemaphoreType.DMA((count,)),
        ],
        compiler_params=pltpu.CompilerParams(
            collective_id=0, has_side_effects=True, vmem_limit_bytes=60 * 1024 * 1024
        ),
        name="block_backward",
    )(out_cotangent[0], value_pre[0], gate_pre[0], out_weight, packed)
    small = jnp.transpose(small, (1, 0, 2)).reshape(KP, C // S)
    return grad_value[None], grad_gate[None], grad_weight, small[:K], small[K]


def solution(mesh):
    placed = (
        P("dp", "sp", None),
        P("dp", "sp", None),
        P("dp", "sp", None),
        P("dp", None),
        P(None, "sp"),
        P("sp"),
    )
    return jax.shard_map(
        shards,
        mesh=mesh,
        in_specs=placed,
        out_specs=(
            P("dp", "sp", None),
            P("dp", "sp", None),
            P(("sp", "dp"), None),
            P(None, "sp"),
            P("sp"),
        ),
        check_vma=False,
    )
```

time: 357 us -> 164 us (0.46)
  waiting for transfers between devices: 180 us -> 0 us
  Pallas kernels: 0 us -> 154 us
  blocking collectives: 76.8 us -> 0 us
  other arithmetic: 47.5 us -> 0.62 us
  matrix products: 18.1 us -> 0 us
  between operations: 14.8 us -> 0.67 us
  starting transfers between devices: 7.62 us -> 0 us
    reduce_scatter x2 -> x0, waiting for transfers between devices: 179 us -> none  [the longest x1 171 us: shards(): lax.psum_scatter(lax.dot_general(activation, cotangent, (((0,), (0,)), ((...]
    pallas_call x0 -> x1, Pallas kernels: none -> 154 us  [shards(): pl.pallas_call(functools.partial(block_kernel, S, N, T, C, K, HB, ids), o...]
    all_gather x2 -> x0, blocking collectives: 44.9 us -> none  [the longest x1 25.9 us: shards(): lax.all_gather(conv_kernel, 'sp', axis=1, tiled=True)]
    reduce_sum x3 -> x0, other arithmetic: 23.4 us -> none  [the longest x1 11.8 us: mechanism(): jnp.sum(conv, axis=1)]
    broadcast_in_dim x2 -> x0, other arithmetic: 19.6 us -> none  [the longest x1 18 us: shards(): grad_gates[None]]
    dot_general x2 -> x0, matrix products: 18.1 us -> none  [the longest x1 10 us: shards(): lax.dot_general(activation, cotangent, (((0,), (0,)), ((), ())), preferre...]
    unnamed x1 -> x0, blocking collectives: 17.5 us -> none
    psum x1 -> x0, blocking collectives: 14.4 us -> none  [shards(): kernel_sum, gain_sum = lax.psum((kernel_part, gain_part), 'dp')]
  transfers between devices with their start and end apart: 5 -> 0, of which waited for: 2 -> 0; matrix products, arithmetic and copies ran while one was open for 13% -> 0% of each run, Pallas kernels for 0% -> 0%
where the time goes in v1:
time: 164 us
  Pallas kernels  154 us (94%)
  local copies, waits for them, and re-layouts  8.3 us (5%)
    pallas_call x1, Pallas kernels, shards(): pl.pallas_call(functools.partial(block_kernel, S, N, T, C, K, HB, ids), o...  154 us
    unnamed x9, local copies, waits for them, and re-layouts  4.76 us

profile of v1, /device:TPU:14, one launch (start us, length us, event | category | flops | bytes accessed | tf_op | source)
XLA Modules:
  0.0 163.8 jit_solution(1871818188825652326)
XLA Ops:
  0.6 0.7 copy.12
  1.3 0.7 concatenate.8
  2.0 0.6 maximum_bitcast_fusion.taps
  2.7 154.2 %block_backward.1 = (bf16[256,2048]{1,0:T(8,128)(2,1)}, bf16[256,2048]{1,0:T(8,128)(2,1)}, f32[64,2048]{1,0:T(8,128)}, f32[2,32,128]{2,1,0:T(8,128)}) custom-call(bf16[256,2048]{1,0:T(8,128)(2,1)} %bitcast.14, bf16[256,2048]{1,0:T(8,128)(2,1)} %bitcast.15, bf16[256,2048]{1,0:T(8,128)(2,1)} %bitcast.16, bf16[512,2048]{1,0:T(8,128)(2,1)} %w.1, ...), custom_call_target="tpu_custom_call" | custom-call | tf_op jit(solution)/shard_map/block_backward/pallas_call | solution.py:326
  156.9 0.0 copy-start
  156.9 1.3 slice.14
  158.3 0.8 copy.13
  159.1 0.6 copy.14
  159.7 0.0 copy-start.1
  159.7 2.4 %copy.18 = bf16[1,256,2048]{2,1,0:T(8,128)(2,1)} copy(bf16[1,256,2048]{2,1,0:T(8,128)(2,1)} %bitcast.18) | data formatting | bytes 2097152
  162.0 0.0 copy-done
  162.1 1.0 copy.19
  163.0 0.0 copy-done.1
  163.0 0.8 copy.20
  (2 shorter events, 0.0 us)
Async XLA Ops:
  156.9 5.2 %copy-start = (bf16[256,2048]{1,0:T(8,128)(2,1)S(1)}, bf16[256,2048]{1,0:T(8,128)(2,1)}, u32[]{:S(2)}) copy-start(bf16[256,2048]{1,0:T(8,128)(2,1)} %get-tuple-element.10) | copy-start | bytes 3145732
  159.7 3.3 %copy-start.1 = (f32[64,2048]{1,0:T(8,128)S(1)}, f32[64,2048]{1,0:T(8,128)}, u32[]{:S(2)}) copy-start(f32[64,2048]{1,0:T(8,128)} %get-tuple-element.20) | copy-start | bytes 1572868

commit v2 on v1

--- a/solution.py
+++ b/solution.py
@@ -17,7 +17,7 @@
 def block_kernel(
     S, N, T, C, K, HB, ids,
     cot, val, gate, w, taps,
-    gv, gg, gw, kout,
+    gv, gg, gw, kout, gout,
     cot_all, ext, cen, gc, gext, kall, act, act_all, ga_send, ga, wpart, rbuf,
     kg, krecv, ksum, k2recv, send_sem, recv_sem,
 ):
@@ -190,16 +190,19 @@
             device_id_type=pl.DeviceIdType.MESH,
         )
 
-    for j in range(S):
-        owner, rows, c = block_of(j)
-
-        @pl.when(owner != me)
-        def _():
-            c.start()
-
-        @pl.when(owner == me)
-        def _():
-            rbuf[s] = wpart[rows, :]
+    def send_blocks(first, last):
+        for j in range(first, last):
+            owner, rows, c = block_of(j)
+
+            @pl.when(owner != me)
+            def _():
+                c.start()
+
+            @pl.when(owner == me)
+            def _():
+                rbuf[s] = wpart[rows, :]
+
+    send_blocks(0, S // 2)
 
     for j in range(1, N // 2):
         arrived(ga.at[pl.ds(lax.rem(d + 2 * j, N) * cpd, cpd)], ids["ga"] + 2 * j)
@@ -243,6 +246,7 @@
     for j in range(1, S):
         to = lax.rem(s + j, S)
         send(kg.at[pl.ds(to * cps, cps)], krecv.at[j], ids["kg"] + j, to, d)
+    send_blocks(S // 2, S)
 
     arrived(gext.at[:, pl.ds(T, HB), :], ids["back"])
 
@@ -276,7 +280,10 @@
     for j in range(1, N):
         arrived(k2recv.at[j], ids["k2"] + j)
         acc = acc + k2recv[j]
-    kout[...] = acc * factor
+    for c in range(cps):
+        cols = slice(c * LANES, (c + 1) * LANES)
+        kout[:, cols] = (acc[c] * factor)[:K]
+        gout[:, cols] = (acc[c] * factor)[K : K + 1]
 
     home = me // S
     for q in range(S):
@@ -323,16 +330,17 @@
         ids[name] = count
         count += size
     vm = pl.BlockSpec(memory_space=pltpu.VMEM)
-    grad_value, grad_gate, grad_weight, small = pl.pallas_call(
+    grad_value, grad_gate, grad_weight, grad_taps, grad_gain = pl.pallas_call(
         functools.partial(block_kernel, S, N, T, C, K, HB, ids),
         out_shape=(
             jax.ShapeDtypeStruct((T, C), bf16),
             jax.ShapeDtypeStruct((T, C), bf16),
             jax.ShapeDtypeStruct((block, C), f32),
-            jax.ShapeDtypeStruct((cps, KP, LANES), f32),
+            jax.ShapeDtypeStruct((K, C // S), f32),
+            jax.ShapeDtypeStruct((1, C // S), f32),
         ),
         in_specs=[vm] * 5,
-        out_specs=(vm,) * 4,
+        out_specs=(vm,) * 5,
         scratch_shapes=[
             pltpu.VMEM((N, T, C), bf16),
             pltpu.VMEM((chunks, T + HB, LANES), f32),
@@ -358,8 +366,7 @@
         ),
         name="block_backward",
     )(out_cotangent[0], value_pre[0], gate_pre[0], out_weight, packed)
-    small = jnp.transpose(small, (1, 0, 2)).reshape(KP, C // S)
-    return grad_value[None], grad_gate[None], grad_weight, small[:K], small[K]
+    return grad_value[None], grad_gate[None], grad_weight, grad_taps, grad_gain[0]
 
 
 def solution(mesh):

time: 164 us -> 158 us (0.963)
  the two profiles are of different devices: /device:TPU:14 before, /device:TPU:3 now
where the time goes in v2:
time: 158 us
  Pallas kernels  150 us (95%)
  local copies, waits for them, and re-layouts  6.78 us (4%)
    pallas_call x1, Pallas kernels, shards(): pl.pallas_call(functools.partial(block_kernel, S, N, T, C, K, HB, ids), o...  150 us
    unnamed x13, local copies, waits for them, and re-layouts  5.38 us

profile of v2, /device:TPU:3, one launch (start us, length us, event | category | flops | bytes accessed | tf_op | source)
XLA Modules:
  0.0 157.8 jit_solution(13228991260276887878)
XLA Ops:
  0.6 0.7 copy.12
  1.3 0.7 concatenate.8
  2.0 0.6 maximum_bitcast_fusion.taps
  2.7 149.8 %block_backward.1 = (bf16[256,2048]{1,0:T(8,128)(2,1)}, bf16[256,2048]{1,0:T(8,128)(2,1)}, f32[64,2048]{1,0:T(8,128)}, f32[31,256]{1,0:T(8,128)}, f32[1,256]{1,0:T(1,128)}) custom-call(bf16[256,2048]{1,0:T(8,128)(2,1)} %bitcast.9, bf16[256,2048]{1,0:T(8,128)(2,1)} %bitcast.10, bf16[256,2048]{1,0:T(8,128)(2,1)} %bitcast.11, bf16[512,2048]{1,0:T(8,128)(2,1)} %w.1, ...), custom_call_target="tpu_custom_call" | custom-call | tf_op jit(solution)/shard_map/block_backward/pallas_call | solution.py:333
  152.4 0.0 copy-start
  152.4 0.0 copy-start.1
  152.5 2.4 %copy.18 = bf16[1,256,2048]{2,1,0:T(8,128)(2,1)} copy(bf16[1,256,2048]{2,1,0:T(8,128)(2,1)} %bitcast.13) | data formatting | bytes 2097152
  154.9 0.0 copy-done
  154.9 0.0 copy-start.2
  154.9 0.0 copy-start.3
  154.9 1.0 copy.19
  155.9 0.0 copy-done.1
  155.9 0.8 copy.20
  156.7 0.0 copy-done.2
  156.7 0.6 copy.21
  157.3 0.0 copy-done.3
  157.3 0.6 copy.22
  (1 shorter events, 0.0 us)
Async XLA Ops:
  152.4 2.4 %copy-start = (bf16[256,2048]{1,0:T(8,128)(2,1)S(1)}, bf16[256,2048]{1,0:T(8,128)(2,1)}, u32[]{:S(2)}) copy-start(bf16[256,2048]{1,0:T(8,128)(2,1)} %get-tuple-element.11) | copy-start | bytes 3145732
  152.4 3.4 %copy-start.1 = (f32[64,2048]{1,0:T(8,128)S(1)}, f32[64,2048]{1,0:T(8,128)}, u32[]{:S(2)}) copy-start(f32[64,2048]{1,0:T(8,128)} %get-tuple-element.22) | copy-start | bytes 1572868
  154.9 1.8 %copy-start.2 = (f32[31,256]{1,0:T(8,128)S(1)}, f32[31,256]{1,0:T(8,128)}, u32[]{:S(2)}) copy-start(f32[31,256]{1,0:T(8,128)} %get-tuple-element.23) | copy-start | bytes 95236
  154.9 2.4 %copy-start.3 = (f32[1,256]{1,0:T(1,128)S(1)}, f32[1,256]{1,0:T(1,128)}, u32[]{:S(2)}) copy-start(f32[1,256]{1,0:T(1,128)} %get-tuple-element.14) | copy-start | bytes 3076
